TPU v7x, 32 devices: a whole 2x2x4 slice. The times are simulated.
32 devices in a mesh: sp: 8 (over z, y), tp: 4 (over x, core).
Axes of the slice: x: 2, y: 2, z: 4, core: 2. Of those that a mesh axis runs over, the one named last changes fastest.
Arguments:
- hidden: bfloat16 [2048, 4096], P('sp'), as said below
- key_weight: bfloat16 [4096, 1024], P(None, 'tp'), as said below
- queries: bfloat16 [2048, 4096], P('sp', 'tp'), as said below
- values: bfloat16 [2048, 1024], P('sp', 'tp'), as said below
- map_out: bfloat16 [2048, 8192], P('sp', 'tp'), as said below
- log_sums: float32 [32, 2048], P('tp', 'sp'), as said below
- out_grad: bfloat16 [2048, 4096], P('sp', 'tp'), may hold values from -6 to 6
- mixing: float32 [16], P('tp'), may hold values from 0.3 to 0.8
- out_gain: float32 [256], replicated, may hold values from 0.1 to 1.9
Outputs:
- grad_query: bfloat16 [2048, 4096], P('sp', 'tp')
- grad_key: bfloat16 [2048, 1024], P('sp', 'tp')
- grad_value: bfloat16 [2048, 1024], P('sp', 'tp')
- grad_weight: float32 [4096, 1024], P('sp', 'tp')
Inputs may be any that keep to these rules, and one draw needn't show every extreme that they name: `hidden`: inputs of order one. `key_weight`: entries of order 1 / sqrt(4096) times a constant. `queries`: entries of order one. `values`: entries of order one. `map_out`: for head h and map m: the row's weights exp(scores - log_sums) over keys j <= i times the values of key head g(h), rounded to bfloat16.
All inputs are finite; a program needn't handle non-finite values.
Results may differ from a plain program's by a relative error of at most 0.02.
Values may be sent and summed in bfloat16 or wider, within the bound.
A program may use at most 256 MiB of HBM per device.

v0:
```python
import jax
import jax.numpy as jnp
from jax import lax
from jax.sharding import PartitionSpec as P

HEAD_DIM = 128
V_DIM = 256


OUT_SCALE = 0.8
NORM_EPS = 1e-06


def shifted(value, axis, steps):
    count = lax.axis_size(axis)
    pairs = [(source, (source + steps) % count) for source in range(count)]
    return lax.ppermute(value, axis, pairs)


def head_terms(out_grad, map_out, mixing, out_gain):
    rows_here = out_grad.shape[0]
    heads_here = mixing.shape[0]
    v_width = out_gain.shape[0]
    maps_out = map_out.astype(jnp.float32).reshape(rows_here, heads_here, 2, v_width)
    pre_norm = maps_out[:, :, 0] - mixing[None, :, None] * maps_out[:, :, 1]
    inverse = lax.rsqrt(jnp.mean(pre_norm * pre_norm, axis=-1, keepdims=True) + NORM_EPS)
    upstream = (
        out_grad.astype(jnp.float32).reshape(rows_here, heads_here, v_width) * out_gain * OUT_SCALE
    )
    d_out = inverse * (
        upstream
        - pre_norm * inverse * inverse * jnp.mean(upstream * pre_norm, axis=-1, keepdims=True)
    )
    row_terms = jnp.sum(d_out[:, :, None, :] * maps_out, axis=-1).reshape(rows_here, heads_here * 2)
    return (d_out.reshape(rows_here, heads_here * v_width).astype(jnp.bfloat16), row_terms)


def block_grads(query_blk, d_blk, stats_blk, query_pos, key_part, value_part, key_pos, mix_blk):
    n_rows, n_groups, per_group = (query_blk.shape[0], query_blk.shape[1], query_blk.shape[2])
    scale = query_blk.shape[-1] ** (-0.5)
    stat_cols = 2 * n_groups * per_group
    log_part = jnp.transpose(
        stats_blk[:, :stat_cols].reshape(n_rows, n_groups, per_group, 2), (1, 2, 3, 0)
    )[..., None]
    term_part = jnp.transpose(
        stats_blk[:, stat_cols:].reshape(n_rows, n_groups, per_group, 2), (1, 2, 3, 0)
    )[..., None]
    scores = (
        jnp.einsum("rgpmd,kgmd->gpmrk", query_blk, key_part, preferred_element_type=jnp.float32)
        * scale
    )
    visible = key_pos[None, :] <= query_pos[:, None]
    probs_map = jnp.exp(jnp.where(visible, scores - log_part, -1e30))
    d_attn = jnp.einsum("rgpv,kgv->gprk", d_blk, value_part, preferred_element_type=jnp.float32)
    mix_cols = mix_blk[:, :, None, None]
    weights_a = (probs_map[:, :, 0] - mix_cols * probs_map[:, :, 1]).astype(jnp.bfloat16)
    d_scores = jnp.stack(
        [
            probs_map[:, :, 0] * (d_attn - term_part[:, :, 0]),
            -mix_cols * probs_map[:, :, 1] * (d_attn - term_part[:, :, 1]),
        ],
        axis=2,
    ).astype(jnp.bfloat16)
    grad_q = (
        jnp.einsum("gpmrk,kgmd->rgpmd", d_scores, key_part, preferred_element_type=jnp.float32)
        * scale
    )
    grad_k = (
        jnp.einsum("gpmrk,rgpmd->kgmd", d_scores, query_blk, preferred_element_type=jnp.float32)
        * scale
    )
    grad_v = jnp.einsum("gprk,rgpv->kgv", weights_a, d_blk, preferred_element_type=jnp.float32)
    return (grad_q, grad_k, grad_v)


def on_device(hidden, key_weight, queries, values, map_out, log_sums, out_grad, mixing, out_gain):
    n_rows = queries.shape[0]
    heads_here = mixing.shape[0]
    groups_here = values.shape[1] // V_DIM
    per_group = heads_here // groups_here
    sp_count = lax.axis_size("sp")
    sp_index = lax.axis_index("sp")
    key_rows = jnp.dot(hidden, key_weight, preferred_element_type=jnp.float32).astype(jnp.bfloat16)
    d_rows, row_terms = head_terms(out_grad, map_out, mixing, out_gain)
    stats = jnp.concatenate([log_sums.T, row_terms], axis=1)
    positions = sp_index * n_rows + jnp.arange(n_rows, dtype=jnp.int32)
    mix_blk = mixing.reshape(groups_here, per_group)
    k_cols = key_rows.shape[1]
    v_cols = values.shape[1]
    q_cols = queries.shape[1]
    query_blk = queries.reshape(n_rows, groups_here, per_group, 2, HEAD_DIM)
    d_blk = d_rows.reshape(n_rows, groups_here, per_group, V_DIM)

    def block_terms(key_piece, value_piece, start):
        n_keys = key_piece.shape[0]
        key_pos = start + jnp.arange(n_keys, dtype=jnp.int32)
        grad_q, grad_k, grad_v = block_grads(
            query_blk,
            d_blk,
            stats,
            positions,
            key_piece.reshape(n_keys, groups_here, 2, HEAD_DIM),
            value_piece.reshape(n_keys, groups_here, V_DIM),
            key_pos,
            mix_blk,
        )
        return (
            grad_q.reshape(n_rows, q_cols),
            grad_k.reshape(n_keys, k_cols),
            grad_v.reshape(n_keys, v_cols),
        )

    def cycle_step(step, state):
        grad_acc, kv_now, grads_now = state
        owner = (sp_index - step + sp_count) % sp_count
        start = owner * n_rows

        def active(inner):
            acc_q, acc_kv = inner
            grad_q, grad_k, grad_v = block_terms(kv_now[:, :k_cols], kv_now[:, k_cols:], start)
            return (acc_q + grad_q, acc_kv + jnp.concatenate([grad_k, grad_v], axis=1))

        def passive(inner):
            return inner

        grad_acc, grads_now = lax.cond(
            start <= positions[-1], active, passive, (grad_acc, grads_now)
        )
        kv_now = shifted(kv_now, "sp", 1)
        grads_now = shifted(grads_now, "sp", 1)
        return (grad_acc, kv_now, grads_now)

    init = (
        jnp.zeros((n_rows, q_cols), jnp.float32),
        jnp.concatenate([key_rows, values], axis=1),
        jnp.zeros((n_rows, k_cols + v_cols), jnp.float32),
    )
    grad_acc, kv_last, grads_last = lax.fori_loop(0, sp_count, cycle_step, init)
    key_own = grads_last[:, :k_cols]
    value_own = grads_last[:, k_cols:]
    grad_key = key_own.astype(jnp.bfloat16)
    grad_value = value_own.astype(jnp.bfloat16)
    grad_query = grad_acc.astype(jnp.bfloat16)
    grad_weight = lax.psum_scatter(
        lax.dot_general(
            hidden, grad_key, (((0,), (0,)), ((), ())), preferred_element_type=jnp.float32
        ).astype(jnp.bfloat16),
        "sp",
        scatter_dimension=0,
        tiled=True,
    ).astype(jnp.float32)
    return (grad_query, grad_key, grad_value, grad_weight)


def solution(mesh):
    placed = (
        P("sp", None),
        P(None, "tp"),
        P("sp", "tp"),
        P("sp", "tp"),
        P("sp", "tp"),
        P("tp", "sp"),
        P("sp", "tp"),
        P("tp"),
        P(),
    )
    return jax.shard_map(
        on_device,
        mesh=mesh,
        in_specs=placed,
        out_specs=(P("sp", "tp"), P("sp", "tp"), P("sp", "tp"), P("sp", "tp")),
        check_vma=False,
    )
```

profile of v0, /device:TPU:0, one launch (start us, length us, event | category | flops | bytes accessed | tf_op | source)
XLA Modules:
  0.0 365.3 jit_solution(10300057568519587279)
XLA Ops:
  7.2 1.6 copy.138
  8.9 1.5 fusion.33
  10.4 2.6 copy.166
  13.0 2.5 copy.167
  15.5 2.0 copy.141
  17.5 2.1 convert_element_type.46
  19.7 2.6 copy.144
  22.2 2.5 copy.145
  24.9 2.4 multiply_reduce_fusion.2
  27.6 1.4 fusion.31
  29.0 2.6 copy.147
  31.6 1.5 multiply_reduce_fusion
  33.7 1.2 copy.137
  35.9 2.6 convolution_convert_fusion.1
  39.3 2.0 fusion.24
  41.3 1.0 broadcast_in_dim.12
  42.4 243.4 %while.19 = (s32[]{:T(128)}, f32[256,1024]{0,1:T(8,128)}, bf16[256,512]{1,0:T(8,128)(2,1)}, f32[256,512]{0,1:T(8,128)S(1)}, s32[]{:T(128)}, /*index=5*/s32[256]{...) while((s32[]{:T(128)}, f32[256,1024]{0,1:T(8,128)}, ...), condition=%wide.region_6.7_spmd, body=%wide.region_3.6_spmd.sunk | while | flops 678822144 | bytes 36507880 | solution.py:138
  42.4 1.0 copy.183
  43.3 1.3 slice.80
  45.3 10.1 %conditional.2 = ((f32[256,1024]{0,1:T(8,128)}, f32[256,512]{0,1:T(8,128)S(1)})) conditional(s32[]{:T(128)} %convert_element_type.61, (f32[256,1024]{0,1:T(8,128)}, f32[256,512]{0,1:T(8,128)S(1)}) %tuple.69, (s32[]{:T(128)}, s32[256]{0:T(256)}, bf16[256,512]{1,0:T(8,128)(2,1)S(1)}, bf16[256,1,4,2,128]{0,4,2,3,1:T(8,128)(2,1)}, f32[256,8]{0,1:T(8,128)}, ...), branch_computations={%region_4.4_spmd, %region_5.5_spmd} | conditional | flops 678822144 | bytes 31788796 | solution.py:126
  47.0 1.4 broadcast_compare_fusion
  49.2 1.7 fusion.1
  55.3 3.0 collective-permute-start.1
  58.3 1.5 collective-permute-start
  59.8 14.4 %collective-permute-done.1 = f32[256,512]{0,1:T(8,128)} collective-permute-done((f32[256,512]{0,1:T(8,128)S(1)}, f32[256,512]{0,1:T(8,128)}, u32[]{:S(2)}, u32[]{:S(2)}) %collective-permute-start.1) | collective-permute-done | bytes 524320 | tf_op jit(solution)/shard_map/while/body/eval_jaxpr/ppermute | solution.py:17
  74.2 1.0 copy.188
  75.3 3.7 %collective-permute-done = bf16[256,512]{1,0:T(8,128)(2,1)} collective-permute-done((bf16[256,512]{1,0:T(8,128)(2,1)S(1)}, bf16[256,512]{1,0:T(8,128)(2,1)}, u32[]{:S(2)}, u32[]{:S(2)}) %collective-permute-start) | collective-permute-done | bytes 262176 | tf_op jit(solution)/shard_map/while/body/eval_jaxpr/ppermute | solution.py:17
  80.0 1.3 slice.80
  81.9 8.8 %collective-permute-start.1 = (f32[256,512]{0,1:T(8,128)S(1)}, f32[256,512]{0,1:T(8,128)}, u32[]{:S(2)}, u32[]{:S(2)}) collective-permute-start(f32[256,512]{0,1:T(8,128)S(1)} %get-tuple-element.522), channel_id=1, source_target_pairs={{0,4},{4,8},{8,12},{12,16},{16,20},{20,24},{24,28},{28,0},{1,5},{5... | collective-permute-start | bytes 1572872 | tf_op jit(solution)/shard_map/while/body/eval_jaxpr/ppermute | solution.py:17
  90.6 2.4 collective-permute-start
  93.1 13.5 %collective-permute-done.1 = f32[256,512]{0,1:T(8,128)} collective-permute-done((f32[256,512]{0,1:T(8,128)S(1)}, f32[256,512]{0,1:T(8,128)}, u32[]{:S(2)}, u32[]{:S(2)}) %collective-permute-start.1) | collective-permute-done | bytes 524320 | tf_op jit(solution)/shard_map/while/body/eval_jaxpr/ppermute | solution.py:17
  106.6 1.0 copy.188
  107.6 2.9 collective-permute-done
  111.4 1.3 slice.80
  113.4 12.0 %collective-permute-start = (bf16[256,512]{1,0:T(8,128)(2,1)S(1)}, bf16[256,512]{1,0:T(8,128)(2,1)}, u32[]{:S(2)}, u32[]{:S(2)}) collective-permute-start(bf16[256,512]{1,0:T(8,128)(2,1)S(1)} %copy.183), channel_id=1, source_target_pairs={{0,4},{4,8},{8,12},{12,16},{16,20},{20,24},{24,28},{28,0},{1,5},{5... | collective-permute-start | bytes 786440 | tf_op jit(solution)/shard_map/while/body/eval_jaxpr/ppermute | solution.py:17
  125.4 12.6 %collective-permute-done.1 = f32[256,512]{0,1:T(8,128)} collective-permute-done((f32[256,512]{0,1:T(8,128)S(1)}, f32[256,512]{0,1:T(8,128)}, u32[]{:S(2)}, u32[]{:S(2)}) %collective-permute-start.1) | collective-permute-done | bytes 524320 | tf_op jit(solution)/shard_map/while/body/eval_jaxpr/ppermute | solution.py:17
  138.0 1.0 copy.188
  139.1 2.0 collective-permute-done
  142.1 1.3 slice.80
  144.1 2.9 collective-permute-start
  147.0 21.9 %collective-permute-done.1 = f32[256,512]{0,1:T(8,128)} collective-permute-done((f32[256,512]{0,1:T(8,128)S(1)}, f32[256,512]{0,1:T(8,128)}, u32[]{:S(2)}, u32[]{:S(2)}) %collective-permute-start.1) | collective-permute-done | bytes 524320 | tf_op jit(solution)/shard_map/while/body/eval_jaxpr/ppermute | solution.py:17
  168.9 1.0 copy.188
  169.9 1.8 collective-permute-done
  172.6 1.3 slice.80
  174.7 24.0 %collective-permute-done.1 = f32[256,512]{0,1:T(8,128)} collective-permute-done((f32[256,512]{0,1:T(8,128)S(1)}, f32[256,512]{0,1:T(8,128)}, u32[]{:S(2)}, u32[]{:S(2)}) %collective-permute-start.1) | collective-permute-done | bytes 524320 | tf_op jit(solution)/shard_map/while/body/eval_jaxpr/ppermute | solution.py:17
  198.7 1.0 copy.188
  199.7 1.8 collective-permute-done
  202.4 1.3 slice.80
  204.5 23.1 %collective-permute-done.1 = f32[256,512]{0,1:T(8,128)} collective-permute-done((f32[256,512]{0,1:T(8,128)S(1)}, f32[256,512]{0,1:T(8,128)}, u32[]{:S(2)}, u32[]{:S(2)}) %collective-permute-start.1) | collective-permute-done | bytes 524320 | tf_op jit(solution)/shard_map/while/body/eval_jaxpr/ppermute | solution.py:17
  227.6 1.0 copy.188
  228.6 1.8 collective-permute-done
  231.4 1.3 slice.80
  233.4 22.3 %collective-permute-done.1 = f32[256,512]{0,1:T(8,128)} collective-permute-done((f32[256,512]{0,1:T(8,128)S(1)}, f32[256,512]{0,1:T(8,128)}, u32[]{:S(2)}, u32[]{:S(2)}) %collective-permute-start.1) | collective-permute-done | bytes 524320 | tf_op jit(solution)/shard_map/while/body/eval_jaxpr/ppermute | solution.py:17
  255.7 1.0 copy.188
  256.7 1.8 collective-permute-done
  259.4 1.3 slice.80
  261.5 21.4 %collective-permute-done.1 = f32[256,512]{0,1:T(8,128)} collective-permute-done((f32[256,512]{0,1:T(8,128)S(1)}, f32[256,512]{0,1:T(8,128)}, u32[]{:S(2)}, u32[]{:S(2)}) %collective-permute-start.1) | collective-permute-done | bytes 524320 | tf_op jit(solution)/shard_map/while/body/eval_jaxpr/ppermute | solution.py:17
  282.9 1.0 copy.188
  284.0 1.8 collective-permute-done
  286.6 2.1 fusion.21
  288.7 1.2 copy-done.3
  289.9 1.0 copy.152
  290.9 65.7 %reduce-scatter.2.cloned.1.call-done = bf16[512,256]{0,1:T(8,128)(2,1)} async-done(((bf16[4096,256]{0,1:T(8,128)(2,1)}), bf16[512,256]{0,1:T(8,128)(2,1)}) %reduce-scatter.2.cloned.1.call-update) | async-done | bytes 262160 | tf_op jit(solution)/shard_map/reduce_scatter | solution.py:144
  356.6 1.9 copy.154
  (81 shorter events, 17.8 us)
Async XLA Ops:
  7.2 28.7 %copy-start = (bf16[256,4096]{1,0:T(8,128)(2,1)S(1)}, bf16[256,4096]{1,0:T(8,128)(2,1)}, u32[]{:S(2)}) copy-start(bf16[256,4096]{1,0:T(8,128)(2,1)} %param.13) | copy-start | bytes 6291460
  7.2 349.4 %reduce-scatter.2.cloned.1.call-start = ((), (), s32[]{:S(2)}) async-start(), calls=%async_computation.1 | async-start | bytes 2359296 | tf_op jit(solution)/shard_map/reduce_scatter | solution.py:144
  19.7 5.1 %copy-start.13 = (f32[256]{0:T(256)S(1)}, f32[256]{0:T(256)}, u32[]{:S(2)}) copy-start(f32[256]{0:T(256)} %param.21) | copy-start | bytes 3076
  19.7 5.1 %copy-start.11 = (f32[4]{0:T(128)S(1)}, f32[4]{0:T(128)}, u32[]{:S(2)}) copy-start(f32[4]{0:T(128)} %param.20) | copy-start | bytes 52
  24.8 2.6 copy-start.4
  24.8 2.6 copy-start.5
  24.8 2.8 copy-start.7
  31.6 4.2 %copy-start.10 = (bf16[256,256]{1,0:T(8,128)(2,1)S(1)}, bf16[256,256]{1,0:T(8,128)(2,1)}, u32[]{:S(2)}) copy-start(bf16[256,256]{1,0:T(8,128)(2,1)} %param.16) | copy-start | bytes 393220
  35.9 3.5 copy-start.6
  49.2 1.7 copy-start.12
  50.9 1.0 copy-start.8
  52.9 1.2 copy-start.1
  54.4 1.0 copy-start.2
  55.3 18.9 %collective-permute-start.1 = (f32[256,512]{0,1:T(8,128)S(1)}, f32[256,512]{0,1:T(8,128)}, u32[]{:S(2)}, u32[]{:S(2)}) collective-permute-start(f32[256,512]{0,1:T(8,128)S(1)} %get-tuple-element.522), channel_id=1, source_target_pairs={{0,4},{4,8},{8,12},{12,16},{16,20},{20,24},{24,28},{28,0},{1,5},{5... | collective-permute-start | bytes 1572872 | tf_op jit(solution)/shard_map/while/body/eval_jaxpr/ppermute | solution.py:17
  58.3 20.7 %collective-permute-start = (bf16[256,512]{1,0:T(8,128)(2,1)S(1)}, bf16[256,512]{1,0:T(8,128)(2,1)}, u32[]{:S(2)}, u32[]{:S(2)}) collective-permute-start(bf16[256,512]{1,0:T(8,128)(2,1)S(1)} %copy.183), channel_id=1, source_target_pairs={{0,4},{4,8},{8,12},{12,16},{16,20},{20,24},{24,28},{28,0},{1,5},{5... | collective-permute-start | bytes 786440 | tf_op jit(solution)/shard_map/while/body/eval_jaxpr/ppermute | solution.py:17
  81.9 24.7 %collective-permute-start.1 = (f32[256,512]{0,1:T(8,128)S(1)}, f32[256,512]{0,1:T(8,128)}, u32[]{:S(2)}, u32[]{:S(2)}) collective-permute-start(f32[256,512]{0,1:T(8,128)S(1)} %get-tuple-element.522), channel_id=1, source_target_pairs={{0,4},{4,8},{8,12},{12,16},{16,20},{20,24},{24,28},{28,0},{1,5},{5... | collective-permute-start | bytes 1572872 | tf_op jit(solution)/shard_map/while/body/eval_jaxpr/ppermute | solution.py:17
  90.6 19.8 %collective-permute-start = (bf16[256,512]{1,0:T(8,128)(2,1)S(1)}, bf16[256,512]{1,0:T(8,128)(2,1)}, u32[]{:S(2)}, u32[]{:S(2)}) collective-permute-start(bf16[256,512]{1,0:T(8,128)(2,1)S(1)} %copy.183), channel_id=1, source_target_pairs={{0,4},{4,8},{8,12},{12,16},{16,20},{20,24},{24,28},{28,0},{1,5},{5... | collective-permute-start | bytes 786440 | tf_op jit(solution)/shard_map/while/body/eval_jaxpr/ppermute | solution.py:17
  113.4 24.7 %collective-permute-start.1 = (f32[256,512]{0,1:T(8,128)S(1)}, f32[256,512]{0,1:T(8,128)}, u32[]{:S(2)}, u32[]{:S(2)}) collective-permute-start(f32[256,512]{0,1:T(8,128)S(1)} %get-tuple-element.522), channel_id=1, source_target_pairs={{0,4},{4,8},{8,12},{12,16},{16,20},{20,24},{24,28},{28,0},{1,5},{5... | collective-permute-start | bytes 1572872 | tf_op jit(solution)/shard_map/while/body/eval_jaxpr/ppermute | solution.py:17
  113.4 27.7 %collective-permute-start = (bf16[256,512]{1,0:T(8,128)(2,1)S(1)}, bf16[256,512]{1,0:T(8,128)(2,1)}, u32[]{:S(2)}, u32[]{:S(2)}) collective-permute-start(bf16[256,512]{1,0:T(8,128)(2,1)S(1)} %copy.183), channel_id=1, source_target_pairs={{0,4},{4,8},{8,12},{12,16},{16,20},{20,24},{24,28},{28,0},{1,5},{5... | collective-permute-start | bytes 786440 | tf_op jit(solution)/shard_map/while/body/eval_jaxpr/ppermute | solution.py:17
  144.0 24.9 %collective-permute-start.1 = (f32[256,512]{0,1:T(8,128)S(1)}, f32[256,512]{0,1:T(8,128)}, u32[]{:S(2)}, u32[]{:S(2)}) collective-permute-start(f32[256,512]{0,1:T(8,128)S(1)} %get-tuple-element.522), channel_id=1, source_target_pairs={{0,4},{4,8},{8,12},{12,16},{16,20},{20,24},{24,28},{28,0},{1,5},{5... | collective-permute-start | bytes 1572872 | tf_op jit(solution)/shard_map/while/body/eval_jaxpr/ppermute | solution.py:17
  144.1 27.6 %collective-permute-start = (bf16[256,512]{1,0:T(8,128)(2,1)S(1)}, bf16[256,512]{1,0:T(8,128)(2,1)}, u32[]{:S(2)}, u32[]{:S(2)}) collective-permute-start(bf16[256,512]{1,0:T(8,128)(2,1)S(1)} %copy.183), channel_id=1, source_target_pairs={{0,4},{4,8},{8,12},{12,16},{16,20},{20,24},{24,28},{28,0},{1,5},{5... | collective-permute-start | bytes 786440 | tf_op jit(solution)/shard_map/while/body/eval_jaxpr/ppermute | solution.py:17
  174.6 24.1 %collective-permute-start.1 = (f32[256,512]{0,1:T(8,128)S(1)}, f32[256,512]{0,1:T(8,128)}, u32[]{:S(2)}, u32[]{:S(2)}) collective-permute-start(f32[256,512]{0,1:T(8,128)S(1)} %get-tuple-element.522), channel_id=1, source_target_pairs={{0,4},{4,8},{8,12},{12,16},{16,20},{20,24},{24,28},{28,0},{1,5},{5... | collective-permute-start | bytes 1572872 | tf_op jit(solution)/shard_map/while/body/eval_jaxpr/ppermute | solution.py:17
  174.6 26.8 %collective-permute-start = (bf16[256,512]{1,0:T(8,128)(2,1)S(1)}, bf16[256,512]{1,0:T(8,128)(2,1)}, u32[]{:S(2)}, u32[]{:S(2)}) collective-permute-start(bf16[256,512]{1,0:T(8,128)(2,1)S(1)} %copy.183), channel_id=1, source_target_pairs={{0,4},{4,8},{8,12},{12,16},{16,20},{20,24},{24,28},{28,0},{1,5},{5... | collective-permute-start | bytes 786440 | tf_op jit(solution)/shard_map/while/body/eval_jaxpr/ppermute | solution.py:17
  204.4 23.2 %collective-permute-start.1 = (f32[256,512]{0,1:T(8,128)S(1)}, f32[256,512]{0,1:T(8,128)}, u32[]{:S(2)}, u32[]{:S(2)}) collective-permute-start(f32[256,512]{0,1:T(8,128)S(1)} %get-tuple-element.522), channel_id=1, source_target_pairs={{0,4},{4,8},{8,12},{12,16},{16,20},{20,24},{24,28},{28,0},{1,5},{5... | collective-permute-start | bytes 1572872 | tf_op jit(solution)/shard_map/while/body/eval_jaxpr/ppermute | solution.py:17
  204.4 26.0 %collective-permute-start = (bf16[256,512]{1,0:T(8,128)(2,1)S(1)}, bf16[256,512]{1,0:T(8,128)(2,1)}, u32[]{:S(2)}, u32[]{:S(2)}) collective-permute-start(bf16[256,512]{1,0:T(8,128)(2,1)S(1)} %copy.183), channel_id=1, source_target_pairs={{0,4},{4,8},{8,12},{12,16},{16,20},{20,24},{24,28},{28,0},{1,5},{5... | collective-permute-start | bytes 786440 | tf_op jit(solution)/shard_map/while/body/eval_jaxpr/ppermute | solution.py:17
  233.3 22.4 %collective-permute-start.1 = (f32[256,512]{0,1:T(8,128)S(1)}, f32[256,512]{0,1:T(8,128)}, u32[]{:S(2)}, u32[]{:S(2)}) collective-permute-start(f32[256,512]{0,1:T(8,128)S(1)} %get-tuple-element.522), channel_id=1, source_target_pairs={{0,4},{4,8},{8,12},{12,16},{16,20},{20,24},{24,28},{28,0},{1,5},{5... | collective-permute-start | bytes 1572872 | tf_op jit(solution)/shard_map/while/body/eval_jaxpr/ppermute | solution.py:17
  233.4 25.1 %collective-permute-start = (bf16[256,512]{1,0:T(8,128)(2,1)S(1)}, bf16[256,512]{1,0:T(8,128)(2,1)}, u32[]{:S(2)}, u32[]{:S(2)}) collective-permute-start(bf16[256,512]{1,0:T(8,128)(2,1)S(1)} %copy.183), channel_id=1, source_target_pairs={{0,4},{4,8},{8,12},{12,16},{16,20},{20,24},{24,28},{28,0},{1,5},{5... | collective-permute-start | bytes 786440 | tf_op jit(solution)/shard_map/while/body/eval_jaxpr/ppermute | solution.py:17
  261.4 21.5 %collective-permute-start.1 = (f32[256,512]{0,1:T(8,128)S(1)}, f32[256,512]{0,1:T(8,128)}, u32[]{:S(2)}, u32[]{:S(2)}) collective-permute-start(f32[256,512]{0,1:T(8,128)S(1)} %get-tuple-element.522), channel_id=1, source_target_pairs={{0,4},{4,8},{8,12},{12,16},{16,20},{20,24},{24,28},{28,0},{1,5},{5... | collective-permute-start | bytes 1572872 | tf_op jit(solution)/shard_map/while/body/eval_jaxpr/ppermute | solution.py:17
  261.5 24.3 %collective-permute-start = (bf16[256,512]{1,0:T(8,128)(2,1)S(1)}, bf16[256,512]{1,0:T(8,128)(2,1)}, u32[]{:S(2)}, u32[]{:S(2)}) collective-permute-start(bf16[256,512]{1,0:T(8,128)(2,1)S(1)} %copy.183), channel_id=1, source_target_pairs={{0,4},{4,8},{8,12},{12,16},{16,20},{20,24},{24,28},{28,0},{1,5},{5... | collective-permute-start | bytes 786440 | tf_op jit(solution)/shard_map/while/body/eval_jaxpr/ppermute | solution.py:17
  286.6 2.1 copy-start.9
  288.6 1.2 copy-start.3
Sparse Core Ops, SparseCore 0:
  288.8 67.7 reduce-scatter.1
where the time goes:
time: 368 us; the launch traced here: 365 us
  waiting for transfers between devices  236 us (64%)
  local copies, waits for them, and re-layouts  58.2 us (16%)
  starting transfers between devices  31.2 us (8%)
  between operations  14.2 us (4%)
  other arithmetic  11.7 us (3%)
  matrix products  7.93 us (2%)
  loops' own time  5.64 us (2%)
    ppermute x16, waiting for transfers between devices, shifted(): return lax.ppermute(value, axis, pairs)  171 us
    reduce_scatter x1, waiting for transfers between devices, on_device(): lax.psum_scatter(lax.dot_general(hidden, grad_key, (((0,), (0,)), ((), ()...  65.7 us
    ppermute x16, starting transfers between devices, shifted(): return lax.ppermute(value, axis, pairs)  31.2 us
    unnamed x31, local copies, waits for them, and re-layouts  13.5 us
    slice x8, local copies, waits for them, and re-layouts, cycle_step(): positions[-1]  10.1 us
    another operation x9, local copies, waits for them, and re-layouts  8.45 us
    while x8, local copies, waits for them, and re-layouts  8.34 us
  transfers between devices with their start and end apart: 17, of which 17 were waited for; matrix products, arithmetic and copies ran while one was open for 3% of the time, Pallas kernels for 0%

commit v1 on v0

v1 whole, which is shorter than its diff:
```python
import functools
import math

import jax
import jax.numpy as jnp
from jax import lax
from jax.experimental import pallas as pl
from jax.experimental.pallas import tpu as pltpu
from jax.sharding import PartitionSpec as P

HEAD_DIM = 128
V_DIM = 256
OUT_SCALE = 0.8
NORM_EPS = 1e-06
LOG2E = math.log2(math.e)
VMEM = pltpu.VMEM


def dot_nn(a, b):
    return lax.dot_general(a, b, (((1,), (0,)), ((), ())), preferred_element_type=jnp.float32)


def dot_nt(a, b):
    return lax.dot_general(a, b, (((1,), (1,)), ((), ())), preferred_element_type=jnp.float32)


def dot_tn(a, b):
    return lax.dot_general(a, b, (((0,), (0,)), ((), ())), preferred_element_type=jnp.float32)


def head_terms(heads, og_ref, mo_ref, mix_ref, gain_ref, d_ref, term_ref):
    gain = gain_ref[...] * OUT_SCALE
    cols = []
    for h in range(heads):
        v_cols = pl.ds(h * V_DIM, V_DIM)
        map_a = mo_ref[:, pl.ds(2 * h * V_DIM, V_DIM)].astype(jnp.float32)
        map_b = mo_ref[:, pl.ds((2 * h + 1) * V_DIM, V_DIM)].astype(jnp.float32)
        pre = map_a - mix_ref[h] * map_b
        inv = lax.rsqrt(jnp.mean(pre * pre, axis=-1, keepdims=True) + NORM_EPS)
        up = og_ref[:, v_cols].astype(jnp.float32) * gain
        d_out = inv * (up - pre * (inv * inv * jnp.mean(up * pre, axis=-1, keepdims=True)))
        d_ref[:, v_cols] = d_out.astype(jnp.bfloat16)
        cols.append(jnp.sum(d_out * map_a, axis=-1, keepdims=True))
        cols.append(jnp.sum(d_out * map_b, axis=-1, keepdims=True))
    rows = cols[0].shape[0]
    lane = lax.broadcasted_iota(jnp.int32, (rows, 128), 1)
    packed = jnp.zeros((rows, 128), jnp.float32)
    for at, col in enumerate(cols):
        packed = jnp.where(lane == at, col, packed)
    term_ref[...] = packed.T[: 2 * heads]


def block_grads(heads, groups, kv, q_ref, d_ref, log_ref, term_ref, mix_ref, gq_ref, masked):
    per_group = heads // groups
    scale = HEAD_DIM ** (-0.5)
    k_cols = groups * 2 * HEAD_DIM
    outs_k, outs_v = [], []
    for g in range(groups):
        keys = [kv[:, (2 * g + m) * HEAD_DIM : (2 * g + m + 1) * HEAD_DIM] for m in range(2)]
        keys_t = [k.T for k in keys]
        vals = kv[:, k_cols + g * V_DIM : k_cols + (g + 1) * V_DIM]
        grad_k = [None, None]
        grad_v = None
        for h in range(g * per_group, (g + 1) * per_group):
            mix = mix_ref[h]
            d_h = d_ref[:, h * V_DIM : (h + 1) * V_DIM]
            d_attn = dot_nt(vals, d_h)
            qs, probs = [], []
            for m in range(2):
                at = 2 * h + m
                q = q_ref[:, at * HEAD_DIM : (at + 1) * HEAD_DIM]
                s = dot_nt(keys[m], q)
                p = jnp.exp2(s * (scale * LOG2E) - log_ref[at : at + 1, :] * LOG2E)
                if masked:
                    k_at = lax.broadcasted_iota(jnp.int32, p.shape, 0)
                    q_at = lax.broadcasted_iota(jnp.int32, p.shape, 1)
                    p = jnp.where(k_at <= q_at, p, 0.0)
                qs.append(q)
                probs.append(p)
            mixed = mix * probs[1]
            w = (probs[0] - mixed).astype(jnp.bfloat16)
            ds = [
                (probs[0] * (d_attn - term_ref[2 * h : 2 * h + 1, :])).astype(jnp.bfloat16),
                (mixed * (term_ref[2 * h + 1 : 2 * h + 2, :] - d_attn)).astype(jnp.bfloat16),
            ]
            for m in range(2):
                at = 2 * h + m
                gq_ref[at * HEAD_DIM : (at + 1) * HEAD_DIM, :] += dot_nn(keys_t[m], ds[m])
                gk = dot_nn(ds[m], qs[m])
                grad_k[m] = gk if grad_k[m] is None else grad_k[m] + gk
            gv = dot_nn(w, d_h)
            grad_v = gv if grad_v is None else grad_v + gv
        outs_k += [gk * scale for gk in grad_k]
        outs_v.append(grad_v)
    return outs_k + outs_v


def store_cols(ref, rows, pieces):
    at = 0
    for piece in pieces:
        ref[rows, at : at + piece.shape[1]] = piece.astype(ref.dtype)
        at += piece.shape[1]


def attend_kernel(
    n, heads, groups,
    kv_ref, q_ref, mo_ref, og_ref, log_ref, gain_ref, mix_ref,
    gq_out, gkv_out,
    d_ref, term_ref, gq_ref,
):
    me = lax.axis_index("sp")
    rows = q_ref.shape[0]
    head_terms(heads, og_ref, mo_ref, mix_ref, gain_ref, d_ref, term_ref)
    gq_ref[...] = jnp.zeros_like(gq_ref)

    def rows_of(j):
        return pl.ds(pl.multiple_of(j * rows, rows), rows)

    def step(j, masked):
        pieces = block_grads(
            heads, groups, kv_ref[rows_of(j), :], q_ref, d_ref, log_ref, term_ref, mix_ref, gq_ref, masked
        )
        store_cols(gkv_out, rows_of(j), pieces)

    step(me, True)

    @pl.loop(0, me)
    def _(j):
        step(j, False)

    @pl.loop(me + 1, n)
    def _(j):
        gkv_out[rows_of(j), :] = jnp.zeros((rows, gkv_out.shape[1]), gkv_out.dtype)

    for at in range(2 * heads):
        cols = slice(at * HEAD_DIM, (at + 1) * HEAD_DIM)
        gq_out[:, cols] = (gq_ref[cols, :] * HEAD_DIM ** (-0.5)).T.astype(gq_out.dtype)


def on_device(n, hidden, key_weight, queries, values, map_out, log_sums, out_grad, mixing, out_gain):
    rows = queries.shape[0]
    heads = mixing.shape[0]
    groups = values.shape[1] // V_DIM
    k_cols = key_weight.shape[1]
    key_rows = jnp.dot(hidden, key_weight, preferred_element_type=jnp.float32).astype(jnp.bfloat16)
    kv = lax.all_gather(jnp.concatenate([key_rows, values], axis=1), "sp", axis=0, tiled=True)
    vm = pl.BlockSpec(memory_space=VMEM)
    grad_query, grad_kv = pl.pallas_call(
        functools.partial(attend_kernel, n, heads, groups),
        out_shape=(
            jax.ShapeDtypeStruct(queries.shape, jnp.bfloat16),
            jax.ShapeDtypeStruct(kv.shape, jnp.bfloat16),
        ),
        in_specs=[vm] * 6 + [pl.BlockSpec(memory_space=pltpu.SMEM)],
        out_specs=(vm, vm),
        scratch_shapes=[
            VMEM((rows, heads * V_DIM), jnp.bfloat16),
            VMEM((2 * heads, rows), jnp.float32),
            VMEM((2 * heads * HEAD_DIM, rows), jnp.float32),
        ],
        compiler_params=pltpu.CompilerParams(vmem_limit_bytes=56 * 2**20),
        cost_estimate=pl.CostEstimate(flops=5 * 10**9, bytes_accessed=10**7, transcendentals=0),
    )(kv, queries, map_out, out_grad, log_sums, out_gain.reshape(1, V_DIM), mixing)
    own = lax.psum_scatter(grad_kv, "sp", scatter_dimension=0, tiled=True)
    grad_key, grad_value = own[:, :k_cols], own[:, k_cols:]
    grad_weight = lax.psum_scatter(
        dot_tn(hidden, grad_key).astype(jnp.bfloat16), "sp", scatter_dimension=0, tiled=True
    ).astype(jnp.float32)
    return grad_query, grad_key, grad_value, grad_weight


def solution(mesh):
    placed = (
        P("sp", None),
        P(None, "tp"),
        P("sp", "tp"),
        P("sp", "tp"),
        P("sp", "tp"),
        P("tp", "sp"),
        P("sp", "tp"),
        P("tp"),
        P(),
    )
    return jax.shard_map(
        functools.partial(on_device, mesh.shape["sp"]),
        mesh=mesh,
        in_specs=placed,
        out_specs=(P("sp", "tp"), P("sp", "tp"), P("sp", "tp"), P("sp", "tp")),
        check_vma=False,
    )
```

time: 368 us -> 229 us (0.62)
  local copies, waits for them, and re-layouts: 58.2 us -> 5.06 us
  waiting for transfers between devices: 236 us -> 198 us
  starting transfers between devices: 31.2 us -> 0.12 us
  other arithmetic: 11.7 us -> 0.72 us
  Pallas kernels: 0 us -> 6.24 us
  loops' own time: 5.64 us -> 0 us
    ppermute x16 -> x0, waiting for transfers between devices: 171 us -> none  [shifted(): return lax.ppermute(value, axis, pairs)]
    reduce_scatter x1 -> x2, waiting for transfers between devices: 65.7 us -> 146 us  [the longest x1 78.2 us: on_device(): own = lax.psum_scatter(grad_kv, 'sp', scatter_dimension=0, tiled=True)]
    all_gather x0 -> x1, waiting for transfers between devices: none -> 51.9 us  [on_device(): lax.all_gather(jnp.concatenate([key_rows, values], axis=1), 'sp', axis=0,...]
    ppermute x16 -> x0, starting transfers between devices: 31.2 us -> none  [shifted(): return lax.ppermute(value, axis, pairs)]
    slice x11 -> x1, local copies, waits for them, and re-layouts: 13.2 us -> 1.64 us  [on_device(): grad_key, grad_value = (own[:, :k_cols], own[:, k_cols:])]
    while x13 -> x0, local copies, waits for them, and re-layouts: 11.1 us -> none
    unnamed x31 -> x7, local copies, waits for them, and re-layouts: 13.5 us -> 3.42 us
    another operation x9 -> x0, local copies, waits for them, and re-layouts: 8.45 us -> none
  transfers between devices with their start and end apart: 17 -> 3, of which waited for: 17 -> 3; matrix products, arithmetic and copies ran while one was open for 3% -> 0% of each run, Pallas kernels for 0% -> 0%
where the time goes in v1:
time: 229 us
  waiting for transfers between devices  198 us (86%)
  between operations  13.8 us (6%)
  Pallas kernels  6.24 us (3%)
  local copies, waits for them, and re-layouts  5.06 us (2%)
  matrix products  4.37 us (2%)
    reduce_scatter x1, waiting for transfers between devices, on_device(): own = lax.psum_scatter(grad_kv, 'sp', scatter_dimension=0, tiled=True)  78.2 us
    reduce_scatter x1, waiting for transfers between devices, on_device(): lax.psum_scatter(dot_tn(hidden, grad_key).astype(jnp.bfloat16), 'sp', sca...  68.1 us
    all_gather x1, waiting for transfers between devices, on_device(): lax.all_gather(jnp.concatenate([key_rows, values], axis=1), 'sp', axis=0,...  51.9 us
    pallas_call x1, Pallas kernels, on_device(): pl.pallas_call(functools.partial(attend_kernel, n, heads, groups), out_sh...  6.24 us
  transfers between devices with their start and end apart: 3, of which 3 were waited for; matrix products, arithmetic and copies ran while one was open for 0% of the time, Pallas kernels for 0%

profile of v1, /device:TPU:0, one launch (start us, length us, event | category | flops | bytes accessed | tf_op | source)
XLA Modules:
  0.0 228.6 jit_solution(3938515674090664108)
XLA Ops:
  7.2 0.0 copy-start
  7.2 0.0 copy-start.2
  7.2 0.0 all-gather.2.cloned.1.call-start
  7.2 1.5 copy-done
  8.8 2.3 %convolution_convert_fusion.1 = bf16[256,256]{1,0:T(8,128)(2,1)S(1)} fusion(bf16[256,4096]{1,0:T(8,128)(2,1)S(1)} %copy-done, bf16[4096,256]{1,0:T(8,128)(2,1)} %param.10), kind=kOutput, calls=%fused_computation.2 | convolution fusion | flops 536936448 | bytes 4325376 | tf_op jit(solution)/shard_map/dot_general | solution.py:145
  11.1 0.0 copy-done.2
  11.1 0.7 pad_maximum_fusion
  11.8 0.0 all-gather.2.cloned.1.call-update
  11.8 0.0 reduce-scatter.3.cloned.1.call-start
  11.9 51.9 %all-gather.2.cloned.1.call-done.kv_ref = bf16[2048,512]{1,0:T(8,128)(2,1)} async-done(((bf16[256,512]{1,0:T(8,128)(2,1)}), bf16[2048,512]{1,0:T(8,128)(2,1)}) %all-gather.2.cloned.1.call-update) | async-done | bytes 2097168 | tf_op jit(solution)/shard_map/all_gather | solution.py:146
  63.8 6.2 %shard_map.120 = (bf16[256,1024]{1,0:T(8,128)(2,1)}, bf16[2048,512]{1,0:T(8,128)(2,1)}) custom-call(bf16[2048,512]{1,0:T(8,128)(2,1)} %all-gather.2.cloned.1.call-done.kv_ref, bf16[256,1024]{1,0:T(8,128)(2,1)} %q_ref.1, bf16[256,2048]{1,0:T(8,128)(2,1)} %mo_ref.1, bf16[256,1024]{1,0:T(8,128)(2,1)} %og_ref.1, f32[8,256]{1,0:T(8,128)} %log_ref.1, ...), custom_call_target="tpu_custom_call" | custom-call | flops 5000000000 | bytes 10000000 | tf_op jit(solution)/shard_map/pallas_call | solution.py:148
  70.0 0.0 reduce-scatter.3.cloned.1.call-update
  70.1 0.0 reduce-scatter.5.cloned.1.call-start
  70.1 78.2 %reduce-scatter.3.cloned.1.call-done = bf16[256,512]{1,0:T(8,128)(2,1)} async-done(((bf16[2048,512]{1,0:T(8,128)(2,1)}), bf16[256,512]{1,0:T(8,128)(2,1)}) %reduce-scatter.3.cloned.1.call-update) | async-done | bytes 262160 | tf_op jit(solution)/shard_map/reduce_scatter | solution.py:164
  148.3 1.6 fusion.1
  150.0 0.0 copy-start.1
  150.0 2.1 fusion
  152.0 0.0 copy-done.1
  152.0 0.0 reduce-scatter.5.cloned.1.call-update
  152.1 68.1 %reduce-scatter.5.cloned.1.call-done = bf16[512,256]{0,1:T(8,128)(2,1)} async-done(((bf16[4096,256]{0,1:T(8,128)(2,1)}), bf16[512,256]{0,1:T(8,128)(2,1)}) %reduce-scatter.5.cloned.1.call-update) | async-done | bytes 262160 | tf_op jit(solution)/shard_map/reduce_scatter | solution.py:166
  220.2 1.9 copy.14
Async XLA Ops:
  7.2 1.6 copy-start
  7.2 3.9 %copy-start.2 = (bf16[256,256]{1,0:T(8,128)(2,1)S(1)}, bf16[256,256]{1,0:T(8,128)(2,1)}, u32[]{:S(2)}) copy-start(bf16[256,256]{1,0:T(8,128)(2,1)} %param.12) | copy-start | bytes 393220
  7.2 56.6 %all-gather.2.cloned.1.call-start = ((), (), s32[]{:S(2)}) async-start(), calls=%async_computation.2 | async-start | bytes 2359296 | tf_op jit(solution)/shard_map/all_gather | solution.py:146
  11.8 136.5 %reduce-scatter.3.cloned.1.call-start = ((), (), s32[]{:S(2)}) async-start(), calls=%async_computation.3 | async-start | bytes 2359296 | tf_op jit(solution)/shard_map/reduce_scatter | solution.py:164
  70.1 150.1 %reduce-scatter.5.cloned.1.call-start = ((), (), s32[]{:S(2)}) async-start(), calls=%async_computation.4 | async-start | bytes 2359296 | tf_op jit(solution)/shard_map/reduce_scatter | solution.py:166
  150.0 2.1 copy-start.1
Sparse Core Ops, SparseCore 0:
  11.9 51.7 all-gather.1
  70.2 78.0 reduce-scatter.2
  152.2 67.9 reduce-scatter.4

commit v2 on v1

--- a/solution.py
+++ b/solution.py
@@ -50,15 +50,14 @@
     term_ref[...] = packed.T[: 2 * heads]
 
 
-def block_grads(heads, groups, kv, q_ref, d_ref, log_ref, term_ref, mix_ref, gq_ref, masked):
+def block_grads(heads, groups, k_ref, v_ref, q_ref, d_ref, log_ref, term_ref, mix_ref, gq_ref, masked):
     per_group = heads // groups
     scale = HEAD_DIM ** (-0.5)
-    k_cols = groups * 2 * HEAD_DIM
     outs_k, outs_v = [], []
     for g in range(groups):
-        keys = [kv[:, (2 * g + m) * HEAD_DIM : (2 * g + m + 1) * HEAD_DIM] for m in range(2)]
+        keys = [k_ref[:, (2 * g + m) * HEAD_DIM : (2 * g + m + 1) * HEAD_DIM] for m in range(2)]
         keys_t = [k.T for k in keys]
-        vals = kv[:, k_cols + g * V_DIM : k_cols + (g + 1) * V_DIM]
+        vals = v_ref[:, g * V_DIM : (g + 1) * V_DIM]
         grad_k = [None, None]
         grad_v = None
         for h in range(g * per_group, (g + 1) * per_group):
@@ -92,77 +91,201 @@
             grad_v = gv if grad_v is None else grad_v + gv
         outs_k += [gk * scale for gk in grad_k]
         outs_v.append(grad_v)
-    return outs_k + outs_v
-
-
-def store_cols(ref, rows, pieces):
-    at = 0
-    for piece in pieces:
-        ref[rows, at : at + piece.shape[1]] = piece.astype(ref.dtype)
-        at += piece.shape[1]
+    return outs_k, outs_v
 
 
 def attend_kernel(
     n, heads, groups,
-    kv_ref, q_ref, mo_ref, og_ref, log_ref, gain_ref, mix_ref,
-    gq_out, gkv_out,
-    d_ref, term_ref, gq_ref,
+    hidden_ref, weight_ref, values_ref, q_ref, mo_ref, og_ref, log_ref, gain_ref, mix_ref,
+    gq_out, gk_out, gv_out,
+    d_ref, term_ref, gq_ref, kv_ref, acc_ref, side_out, side_in, down_out, up_in,
+    kv_recv, kv_up_sem, kv_side_sem, side_send, side_recv, down_send, up_recv,
 ):
     me = lax.axis_index("sp")
-    rows = q_ref.shape[0]
+    outer = n // 2
+    o, y = me // 2, me % 2
+    has_up = o < outer - 1
+    up, down, side = me + 2, me - 2, me + 1 - 2 * y
+
+    def kv_copy(b, part, sems, target, src=None):
+        return pltpu.make_async_remote_copy(
+            src_ref=kv_ref.at[b, part] if src is None else src,
+            dst_ref=kv_ref.at[b, part],
+            send_sem=sems.at[b // 2, part],
+            recv_sem=kv_recv.at[b, part],
+            device_id={"sp": target},
+        )
+
+    def side_copy(ob, part):
+        return pltpu.make_async_remote_copy(
+            src_ref=side_out.at[ob, part],
+            dst_ref=side_in.at[ob, part],
+            send_sem=side_send.at[ob, part],
+            recv_sem=side_recv.at[ob, part],
+            device_id={"sp": side},
+        )
+
+    def down_copy(ob, part):
+        return pltpu.make_async_remote_copy(
+            src_ref=down_out.at[ob, part],
+            dst_ref=up_in.at[ob, part],
+            send_sem=down_send.at[ob, part],
+            recv_sem=up_recv.at[ob, part],
+            device_id={"sp": down},
+        )
+
+    barrier = pltpu.get_barrier_semaphore()
+    pl.semaphore_signal(barrier, inc=1, device_id={"sp": side})
+
+    @pl.when(has_up)
+    def _():
+        pl.semaphore_signal(barrier, inc=1, device_id={"sp": up})
+
+    @pl.when(o > 0)
+    def _():
+        pl.semaphore_signal(barrier, inc=1, device_id={"sp": down})
+
+    pl.semaphore_wait(barrier, 1 + has_up.astype(jnp.int32) + (o > 0).astype(jnp.int32))
+
+    def start_own(part, src=None):
+        @pl.when(has_up)
+        def _():
+            kv_copy(me, part, kv_up_sem, up, src).start()
+
+        @pl.when(y == 0)
+        def _():
+            kv_copy(me, part, kv_side_sem, side, src).start()
+
+    start_own(1, values_ref)
+    kv_ref[me, 0] = dot_nn(hidden_ref[...], weight_ref[...]).astype(jnp.bfloat16)
+    kv_ref[me, 1] = values_ref[...]
+    start_own(0)
     head_terms(heads, og_ref, mo_ref, mix_ref, gain_ref, d_ref, term_ref)
     gq_ref[...] = jnp.zeros_like(gq_ref)
 
-    def rows_of(j):
-        return pl.ds(pl.multiple_of(j * rows, rows), rows)
-
-    def step(j, masked):
-        pieces = block_grads(
-            heads, groups, kv_ref[rows_of(j), :], q_ref, d_ref, log_ref, term_ref, mix_ref, gq_ref, masked
+    def grads(b, masked):
+        return block_grads(
+            heads, groups, kv_ref.at[b, 0], kv_ref.at[b, 1], q_ref, d_ref, log_ref, term_ref, mix_ref, gq_ref, masked
         )
-        store_cols(gkv_out, rows_of(j), pieces)
-
-    step(me, True)
-
-    @pl.loop(0, me)
-    def _(j):
-        step(j, False)
-
-    @pl.loop(me + 1, n)
-    def _(j):
-        gkv_out[rows_of(j), :] = jnp.zeros((rows, gkv_out.shape[1]), gkv_out.dtype)
-
-    for at in range(2 * heads):
-        cols = slice(at * HEAD_DIM, (at + 1) * HEAD_DIM)
-        gq_out[:, cols] = (gq_ref[cols, :] * HEAD_DIM ** (-0.5)).T.astype(gq_out.dtype)
+
+    def store(ref, ob, pieces):
+        for part in range(2):
+            at = 0
+            for piece in pieces[part]:
+                ref[ob, part, :, at : at + piece.shape[1]] = piece.astype(ref.dtype)
+                at += piece.shape[1]
+
+    lag = jnp.where(has_up, o + 2, 2)
+
+    @pl.loop(0, o + lag + 1)
+    def _(t):
+        @pl.when(t == 0)
+        def _():
+            store(acc_ref, o, grads(me, True))
+
+        @pl.when((t > 0) & (t <= o))
+        def _():
+            b = me - 2 * t
+            for part in (1, 0):
+                kv_copy(b, part, kv_up_sem, up).wait_recv()
+
+                @pl.when(has_up)
+                def _():
+                    kv_copy(b, part, kv_up_sem, up).start()
+
+                kv_copy(b, part, kv_side_sem, side).start()
+            store(acc_ref, o - t, grads(b, False))
+
+        @pl.when((t > 0) & (t <= o + 1) & ((t > 1) | (y == 1)))
+        def _():
+            ob = o - t + 1
+            b = 2 * ob + 1 - y
+            for part in (1, 0):
+                kv_copy(b, part, kv_side_sem, side).wait_recv()
+            store(side_out, ob, grads(b, False))
+            for part in range(2):
+                side_copy(ob, part).start()
+
+        @pl.when(t >= lag)
+        def _():
+            ob = o - t + lag
+            for part in range(2):
+                @pl.when((ob < o) | (y == 0))
+                def _():
+                    side_copy(ob, part).wait_recv()
+                    acc_ref[ob, part] += side_in[ob, part].astype(jnp.float32)
+
+                @pl.when(has_up)
+                def _():
+                    down_copy(ob, part).wait_recv()
+                    acc_ref[ob, part] += up_in[ob, part].astype(jnp.float32)
+
+                @pl.when(ob < o)
+                def _():
+                    down_out[ob, part] = acc_ref[ob, part].astype(jnp.bfloat16)
+                    down_copy(ob, part).start()
+
+        @pl.when(t == o + 1)
+        def _():
+            for at in range(2 * heads):
+                cols = slice(at * HEAD_DIM, (at + 1) * HEAD_DIM)
+                gq_out[:, cols] = (gq_ref[cols, :] * HEAD_DIM ** (-0.5)).T.astype(gq_out.dtype)
+
+    gk_out[...] = acc_ref[o, 0].astype(gk_out.dtype)
+    gv_out[...] = acc_ref[o, 1].astype(gv_out.dtype)
+
+    @pl.loop(0, o + 1)
+    def _(ob):
+        for part in range(2):
+            @pl.when(has_up)
+            def _():
+                kv_copy(2 * ob + y, part, kv_up_sem, up).wait_send()
+
+            @pl.when((ob < o) | (y == 0))
+            def _():
+                kv_copy(2 * ob + y, part, kv_side_sem, side).wait_send()
+
+            @pl.when((ob < o) | (y == 1))
+            def _():
+                side_copy(ob, part).wait_send()
+
+            @pl.when(ob < o)
+            def _():
+                down_copy(ob, part).wait_send()
 
 
 def on_device(n, hidden, key_weight, queries, values, map_out, log_sums, out_grad, mixing, out_gain):
     rows = queries.shape[0]
     heads = mixing.shape[0]
-    groups = values.shape[1] // V_DIM
-    k_cols = key_weight.shape[1]
-    key_rows = jnp.dot(hidden, key_weight, preferred_element_type=jnp.float32).astype(jnp.bfloat16)
-    kv = lax.all_gather(jnp.concatenate([key_rows, values], axis=1), "sp", axis=0, tiled=True)
+    width = values.shape[1]
+    groups = width // V_DIM
+    outer = n // 2
     vm = pl.BlockSpec(memory_space=VMEM)
-    grad_query, grad_kv = pl.pallas_call(
+    hops = pltpu.SemaphoreType.DMA((outer, 2))
+    grad_query, grad_key, grad_value = pl.pallas_call(
         functools.partial(attend_kernel, n, heads, groups),
         out_shape=(
             jax.ShapeDtypeStruct(queries.shape, jnp.bfloat16),
-            jax.ShapeDtypeStruct(kv.shape, jnp.bfloat16),
+            jax.ShapeDtypeStruct((rows, width), jnp.bfloat16),
+            jax.ShapeDtypeStruct((rows, width), jnp.bfloat16),
         ),
-        in_specs=[vm] * 6 + [pl.BlockSpec(memory_space=pltpu.SMEM)],
-        out_specs=(vm, vm),
+        in_specs=[vm] * 8 + [pl.BlockSpec(memory_space=pltpu.SMEM)],
+        out_specs=(vm, vm, vm),
         scratch_shapes=[
             VMEM((rows, heads * V_DIM), jnp.bfloat16),
             VMEM((2 * heads, rows), jnp.float32),
             VMEM((2 * heads * HEAD_DIM, rows), jnp.float32),
-        ],
-        compiler_params=pltpu.CompilerParams(vmem_limit_bytes=56 * 2**20),
+            VMEM((n, 2, rows, width), jnp.bfloat16),
+            VMEM((outer, 2, rows, width), jnp.float32),
+        ]
+        + [VMEM((outer, 2, rows, width), jnp.bfloat16)] * 4
+        + [pltpu.SemaphoreType.DMA((n, 2))]
+        + [hops] * 6,
+        compiler_params=pltpu.CompilerParams(
+            vmem_limit_bytes=60 * 2**20, collective_id=0, has_side_effects=True
+        ),
         cost_estimate=pl.CostEstimate(flops=5 * 10**9, bytes_accessed=10**7, transcendentals=0),
-    )(kv, queries, map_out, out_grad, log_sums, out_gain.reshape(1, V_DIM), mixing)
-    own = lax.psum_scatter(grad_kv, "sp", scatter_dimension=0, tiled=True)
-    grad_key, grad_value = own[:, :k_cols], own[:, k_cols:]
+    )(hidden, key_weight, values, queries, map_out, out_grad, log_sums, out_gain.reshape(1, V_DIM), mixing)
     grad_weight = lax.psum_scatter(
         dot_tn(hidden, grad_key).astype(jnp.bfloat16), "sp", scatter_dimension=0, tiled=True
     ).astype(jnp.float32)

time: 229 us -> 155 us (0.68)
  waiting for transfers between devices: 198 us -> 66.3 us
  Pallas kernels: 6.24 us -> 67.7 us
    reduce_scatter x1 -> x0, waiting for transfers between devices: 78.2 us -> none  [on_device(): own = lax.psum_scatter(grad_kv, 'sp', scatter_dimension=0, tiled=True)]
    pallas_call x1, Pallas kernels: 6.24 us -> 67.7 us  [on_device(): pl.pallas_call(functools.partial(attend_kernel, n, heads, groups), out_sh...]
    all_gather x1 -> x0, waiting for transfers between devices: 51.9 us -> none  [on_device(): lax.all_gather(jnp.concatenate([key_rows, values], axis=1), 'sp', axis=0,...]
    dot_general x1 -> x0, matrix products: 2.3 us -> none  [on_device(): jnp.dot(hidden, key_weight, preferred_element_type=jnp.float32)]
  transfers between devices with their start and end apart: 3 -> 1, of which waited for: 3 -> 1; matrix products, arithmetic and copies ran while one was open for 0% -> 0% of each run, Pallas kernels for 0% -> 0%
where the time goes in v2:
time: 155 us
  Pallas kernels  67.7 us (44%)
  waiting for transfers between devices  66.3 us (43%)
  between operations  14.1 us (9%)
  local copies, waits for them, and re-layouts  4 us (3%)
  matrix products  2.98 us (2%)
    pallas_call x1, Pallas kernels, on_device(): pl.pallas_call(functools.partial(attend_kernel, n, heads, groups), out_sh...  67.7 us
    reduce_scatter x1, waiting for transfers between devices, on_device(): lax.psum_scatter(dot_tn(hidden, grad_key).astype(jnp.bfloat16), 'sp', sca...  66.2 us
    unnamed x12, local copies, waits for them, and re-layouts  4 us
  transfers between devices with their start and end apart: 1, of which 1 were waited for; matrix products, arithmetic and copies ran while one was open for 0% of the time, Pallas kernels for 0%

profile of v2, /device:TPU:0, one launch (start us, length us, event | category | flops | bytes accessed | tf_op | source)
XLA Modules:
  0.0 155.1 jit_solution(4347783955584561075)
XLA Ops:
  7.2 0.0 reduce-scatter.2.cloned.1.call-start
  7.2 0.0 copy-start
  7.2 67.7 %shard_map.120 = (bf16[256,1024]{1,0:T(8,128)(2,1)}, bf16[256,256]{1,0:T(8,128)(2,1)}, bf16[256,256]{1,0:T(8,128)(2,1)}) custom-call(bf16[256,4096]{1,0:T(8,128)(2,1)} %hidden_ref.1, bf16[4096,256]{1,0:T(8,128)(2,1)} %weight_ref.1, bf16[256,256]{1,0:T(8,128)(2,1)} %values_ref.1, bf16[256,1024]{1,0:T(8,128)(2,1)} %q_ref.1, bf16[256,2048]{1,0:T(8,128)(2,1)} %mo_ref.1, ...), custom_call_target="tpu_custom_call" | custom-call | flops 5000000000 | bytes 10000000 | tf_op jit(solution)/shard_map/pallas_call | solution.py:265
  75.0 0.0 copy-done
  75.0 3.0 %fusion = bf16[4096,256]{0,1:T(8,128)(2,1)} fusion(bf16[256,256]{1,0:T(8,128)(2,1)} %get-tuple-element.19, bf16[256,4096]{1,0:T(8,128)(2,1)S(1)} %copy-done), kind=kOutput, calls=%fused_computation.1 | convolution fusion | flops 537919488 | bytes 4325376 | tf_op jit(solution)/shard_map/dot_general | solution.py:28
  78.0 0.0 copy-start.2
  78.0 0.0 copy-start.1
  78.0 0.0 copy-start.3
  78.0 0.0 reduce-scatter.2.cloned.1.call-update
  78.0 66.2 %reduce-scatter.2.cloned.1.call-done = bf16[512,256]{0,1:T(8,128)(2,1)} async-done(((bf16[4096,256]{0,1:T(8,128)(2,1)}), bf16[512,256]{0,1:T(8,128)(2,1)}) %reduce-scatter.2.cloned.1.call-update) | async-done | bytes 262160 | tf_op jit(solution)/shard_map/reduce_scatter | solution.py:289
  144.2 1.9 %copy.13 = f32[512,256]{1,0:T(8,128)} copy(bf16[512,256]{0,1:T(8,128)(2,1)} %reduce-scatter.2.cloned.1.call-done) | data formatting | bytes 786432
  146.1 0.0 copy-done.2
  146.1 0.8 copy.17
  146.9 0.0 copy-done.1
  146.9 0.7 copy.18
  147.6 0.0 copy-done.3
  147.6 0.7 copy.19
Async XLA Ops:
  7.2 137.1 %reduce-scatter.2.cloned.1.call-start = ((), (), s32[]{:S(2)}) async-start(), calls=%async_computation.1 | async-start | bytes 2359296 | tf_op jit(solution)/shard_map/reduce_scatter | solution.py:289
  7.2 67.8 %copy-start = (bf16[256,4096]{1,0:T(8,128)(2,1)S(1)}, bf16[256,4096]{1,0:T(8,128)(2,1)}, u32[]{:S(2)}) copy-start(bf16[256,4096]{1,0:T(8,128)(2,1)} %hidden_ref.1) | copy-start | bytes 6291460
  78.0 68.2 %copy-start.2 = (bf16[256,1024]{1,0:T(8,128)(2,1)S(1)}, bf16[256,1024]{1,0:T(8,128)(2,1)}, u32[]{:S(2)}) copy-start(bf16[256,1024]{1,0:T(8,128)(2,1)} %get-tuple-element.18) | copy-start | bytes 1572868
  78.0 69.0 %copy-start.1 = (bf16[256,256]{1,0:T(8,128)(2,1)S(1)}, bf16[256,256]{1,0:T(8,128)(2,1)}, u32[]{:S(2)}) copy-start(bf16[256,256]{1,0:T(8,128)(2,1)} %get-tuple-element.19) | copy-start | bytes 393220
  78.0 69.6 %copy-start.3 = (bf16[256,256]{1,0:T(8,128)(2,1)S(1)}, bf16[256,256]{1,0:T(8,128)(2,1)}, u32[]{:S(2)}) copy-start(bf16[256,256]{1,0:T(8,128)(2,1)} %get-tuple-element.20) | copy-start | bytes 393220
Sparse Core Ops, SparseCore 0:
  78.1 66.0 reduce-scatter.1

commit v3 on v2

--- a/solution.py
+++ b/solution.py
@@ -95,11 +95,12 @@
 
 
 def attend_kernel(
-    n, heads, groups,
+    n, tp_count, heads, groups,
     hidden_ref, weight_ref, values_ref, q_ref, mo_ref, og_ref, log_ref, gain_ref, mix_ref,
-    gq_out, gk_out, gv_out,
-    d_ref, term_ref, gq_ref, kv_ref, acc_ref, side_out, side_in, down_out, up_in,
+    gq_out, gk_out, gv_out, gw_out,
+    d_ref, term_ref, gq_ref, kv_ref, acc_ref, side_out, side_in, down_out, up_in, hid_ref, gk_ref,
     kv_recv, kv_up_sem, kv_side_sem, side_send, side_recv, down_send, up_recv,
+    hid_send, hid_pass, hid_recv, gk_recv, gk_up_sem, gk_down_sem, gk_side_sem,
 ):
     me = lax.axis_index("sp")
     outer = n // 2
@@ -134,18 +135,84 @@
             device_id={"sp": down},
         )
 
+    tp_at = lax.axis_index("tp")
+    rows = q_ref.shape[0]
+    part_rows = rows // tp_count
+    wide = hidden_ref.shape[1] // n
+    own_cols = pl.ds(pl.multiple_of(me * wide, wide), wide)
+    own_rows = pl.ds(pl.multiple_of(tp_at * part_rows, part_rows), part_rows)
+
+    def hid_slice(dest):
+        return pltpu.make_async_remote_copy(
+            src_ref=hidden_ref.at[own_rows, pl.ds(pl.multiple_of(dest * wide, wide), wide)],
+            dst_ref=hid_ref.at[tp_at, me],
+            send_sem=hid_send,
+            recv_sem=hid_recv.at[tp_at],
+            device_id={"sp": dest},
+        )
+
+    def hid_forward(source, target):
+        return pltpu.make_async_remote_copy(
+            src_ref=hid_ref.at[source],
+            dst_ref=hid_ref.at[source],
+            send_sem=hid_pass.at[target],
+            recv_sem=hid_recv.at[source],
+            device_id={"tp": target},
+        )
+
+    def hid_start():
+        @pl.loop(1, n)
+        def _(k):
+            hid_slice((me + k) % n).start()
+
+    def hid_wait(sem):
+        pieces = hid_ref.at[tp_at, pl.ds(0, n - 1)]
+        pltpu.make_async_copy(pieces, pieces, sem).wait()
+
+    def hid_relay():
+        hid_wait(hid_recv.at[tp_at])
+
+        @pl.loop(1, tp_count)
+        def _(k):
+            hid_forward(tp_at, (tp_at + k) % tp_count).start()
+
+    def gk_copy(b, sems, target):
+        return pltpu.make_async_remote_copy(
+            src_ref=gk_ref.at[b],
+            dst_ref=gk_ref.at[b],
+            send_sem=sems.at[b // 2],
+            recv_sem=gk_recv.at[b],
+            device_id={"sp": target},
+        )
+
+    def gk_each(b, act):
+        ob = b // 2
+
+        @pl.when((ob <= o) & has_up)
+        def _():
+            act(gk_copy(b, gk_up_sem, up))
+
+        @pl.when((ob >= o) & (o > 0))
+        def _():
+            act(gk_copy(b, gk_down_sem, down))
+
+        act(gk_copy(b, gk_side_sem, side))
+
+    def add_weight(b):
+        block = jnp.concatenate([hid_ref[k, b] for k in range(tp_count)], axis=0)
+        gw_out[...] += dot_tn(block, gk_ref[b])
+
     barrier = pltpu.get_barrier_semaphore()
-    pl.semaphore_signal(barrier, inc=1, device_id={"sp": side})
-
-    @pl.when(has_up)
-    def _():
-        pl.semaphore_signal(barrier, inc=1, device_id={"sp": up})
-
-    @pl.when(o > 0)
-    def _():
-        pl.semaphore_signal(barrier, inc=1, device_id={"sp": down})
-
-    pl.semaphore_wait(barrier, 1 + has_up.astype(jnp.int32) + (o > 0).astype(jnp.int32))
+
+    @pl.loop(1, n)
+    def _(k):
+        pl.semaphore_signal(barrier, inc=1, device_id={"sp": (me + k) % n})
+
+    @pl.loop(1, tp_count)
+    def _(k):
+        pl.semaphore_signal(barrier, inc=1, device_id={"tp": (tp_at + k) % tp_count})
+
+    pl.semaphore_wait(barrier, n + tp_count - 2)
 
     def start_own(part, src=None):
         @pl.when(has_up)
@@ -160,7 +227,14 @@
     kv_ref[me, 0] = dot_nn(hidden_ref[...], weight_ref[...]).astype(jnp.bfloat16)
     kv_ref[me, 1] = values_ref[...]
     start_own(0)
+    hid_ref[tp_at, me] = hidden_ref[own_rows, own_cols]
+
+    @pl.when(~has_up)
+    def _():
+        hid_start()
+
     head_terms(heads, og_ref, mo_ref, mix_ref, gain_ref, d_ref, term_ref)
+    gw_out[...] = jnp.zeros_like(gw_out)
     gq_ref[...] = jnp.zeros_like(gq_ref)
 
     def grads(b, masked):
@@ -206,6 +280,14 @@
             for part in range(2):
                 side_copy(ob, part).start()
 
+        @pl.when((t == o + 1) & has_up)
+        def _():
+            hid_start()
+
+        @pl.when((t == o + 2) & has_up)
+        def _():
+            hid_relay()
+
         @pl.when(t >= lag)
         def _():
             ob = o - t + lag
@@ -220,6 +302,12 @@
                     down_copy(ob, part).wait_recv()
                     acc_ref[ob, part] += up_in[ob, part].astype(jnp.float32)
 
+                if part == 0:
+                    @pl.when(ob == o)
+                    def _():
+                        gk_ref[me] = acc_ref[o, 0].astype(jnp.bfloat16)
+                        gk_each(me, lambda copy: copy.start())
+
                 @pl.when(ob < o)
                 def _():
                     down_out[ob, part] = acc_ref[ob, part].astype(jnp.bfloat16)
@@ -231,8 +319,44 @@
                 cols = slice(at * HEAD_DIM, (at + 1) * HEAD_DIM)
                 gq_out[:, cols] = (gq_ref[cols, :] * HEAD_DIM ** (-0.5)).T.astype(gq_out.dtype)
 
-    gk_out[...] = acc_ref[o, 0].astype(gk_out.dtype)
+    @pl.when(~has_up)
+    def _():
+        hid_relay()
+
+    gk_out[...] = gk_ref[me]
     gv_out[...] = acc_ref[o, 1].astype(gv_out.dtype)
+
+    @pl.loop(1, tp_count)
+    def _(k):
+        hid_forward((tp_at + k) % tp_count, tp_at).wait_recv()
+
+    add_weight(me)
+
+    @pl.loop(0, outer)
+    def _(k):
+        b = 2 * (outer - 1 - k) + y
+
+        @pl.when(b != me)
+        def _():
+            gk_copy(b, gk_side_sem, side).wait_recv()
+            gk_each(b, lambda copy: copy.start())
+            add_weight(b)
+
+    @pl.loop(0, outer)
+    def _(k):
+        b = 2 * (outer - 1 - k) + 1 - y
+        gk_copy(b, gk_side_sem, side).wait_recv()
+        add_weight(b)
+
+    hid_wait(hid_send)
+
+    @pl.loop(1, tp_count)
+    def _(k):
+        hid_forward(tp_at, (tp_at + k) % tp_count).wait_send()
+
+    @pl.loop(0, outer)
+    def _(ob):
+        gk_each(2 * ob + y, lambda copy: copy.wait_send())
 
     @pl.loop(0, o + 1)
     def _(ob):
@@ -254,7 +378,7 @@
                 down_copy(ob, part).wait_send()
 
 
-def on_device(n, hidden, key_weight, queries, values, map_out, log_sums, out_grad, mixing, out_gain):
+def on_device(n, tp_count, hidden, key_weight, queries, values, map_out, log_sums, out_grad, mixing, out_gain):
     rows = queries.shape[0]
     heads = mixing.shape[0]
     width = values.shape[1]
@@ -262,15 +386,16 @@
     outer = n // 2
     vm = pl.BlockSpec(memory_space=VMEM)
     hops = pltpu.SemaphoreType.DMA((outer, 2))
-    grad_query, grad_key, grad_value = pl.pallas_call(
-        functools.partial(attend_kernel, n, heads, groups),
+    return pl.pallas_call(
+        functools.partial(attend_kernel, n, tp_count, heads, groups),
         out_shape=(
             jax.ShapeDtypeStruct(queries.shape, jnp.bfloat16),
             jax.ShapeDtypeStruct((rows, width), jnp.bfloat16),
             jax.ShapeDtypeStruct((rows, width), jnp.bfloat16),
+            jax.ShapeDtypeStruct((hidden.shape[1] // n, width), jnp.float32),
         ),
         in_specs=[vm] * 8 + [pl.BlockSpec(memory_space=pltpu.SMEM)],
-        out_specs=(vm, vm, vm),
+        out_specs=(vm, vm, vm, vm),
         scratch_shapes=[
             VMEM((rows, heads * V_DIM), jnp.bfloat16),
             VMEM((2 * heads, rows), jnp.float32),
@@ -279,17 +404,19 @@
             VMEM((outer, 2, rows, width), jnp.float32),
         ]
         + [VMEM((outer, 2, rows, width), jnp.bfloat16)] * 4
+        + [
+            VMEM((tp_count, n, rows // tp_count, hidden.shape[1] // n), jnp.bfloat16),
+            VMEM((n, rows, width), jnp.bfloat16),
+        ]
         + [pltpu.SemaphoreType.DMA((n, 2))]
-        + [hops] * 6,
+        + [hops] * 6
+        + [pltpu.SemaphoreType.DMA]
+        + [pltpu.SemaphoreType.DMA((size,)) for size in (tp_count, tp_count, n, outer, outer, outer)],
         compiler_params=pltpu.CompilerParams(
             vmem_limit_bytes=60 * 2**20, collective_id=0, has_side_effects=True
         ),
         cost_estimate=pl.CostEstimate(flops=5 * 10**9, bytes_accessed=10**7, transcendentals=0),
     )(hidden, key_weight, values, queries, map_out, out_grad, log_sums, out_gain.reshape(1, V_DIM), mixing)
-    grad_weight = lax.psum_scatter(
-        dot_tn(hidden, grad_key).astype(jnp.bfloat16), "sp", scatter_dimension=0, tiled=True
-    ).astype(jnp.float32)
-    return grad_query, grad_key, grad_value, grad_weight
 
 
 def solution(mesh):
@@ -305,7 +432,7 @@
         P(),
     )
     return jax.shard_map(
-        functools.partial(on_device, mesh.shape["sp"]),
+        functools.partial(on_device, mesh.shape["sp"], mesh.shape["tp"]),
         mesh=mesh,
         in_specs=placed,
         out_specs=(P("sp", "tp"), P("sp", "tp"), P("sp", "tp"), P("sp", "tp")),

time: 155 us -> 97.9 us (0.63)
  the two profiles are of different devices: /device:TPU:0 before, /device:TPU:29 now
where the time goes in v3:
time: 97.9 us; the launch traced here: 97.7 us
  Pallas kernels  90.2 us (92%)
  local copies, waits for them, and re-layouts  6.87 us (7%)
    pallas_call x1, Pallas kernels, on_device(): pl.pallas_call(functools.partial(attend_kernel, n, tp_count, heads, group...  90.2 us
    unnamed x4, local copies, waits for them, and re-layouts  6.87 us

profile of v3, /device:TPU:29, one launch (start us, length us, event | category | flops | bytes accessed | tf_op | source)
XLA Modules:
  0.0 97.7 jit_solution(403508661896989298)
XLA Ops:
  0.6 90.2 %shard_map.120 = (bf16[256,1024]{1,0:T(8,128)(2,1)}, bf16[256,256]{1,0:T(8,128)(2,1)}, bf16[256,256]{1,0:T(8,128)(2,1)}, f32[512,256]{1,0:T(8,128)}) custom-call(bf16[256,4096]{1,0:T(8,128)(2,1)} %hidden_ref.1, bf16[4096,256]{1,0:T(8,128)(2,1)} %weight_ref.1, bf16[256,256]{1,0:T(8,128)(2,1)} %values_ref.1, bf16[256,1024]{1,0:T(8,128)(2,1)} %q_ref.1, ...), custom_call_target="tpu_custom_call" | custom-call | flops 5000000000 | bytes 10000000 | tf_op jit(solution)/shard_map/pallas_call | solution.py:389
  90.8 1.9 %copy.17 = bf16[256,1024]{1,0:T(8,128)(2,1)} copy(bf16[256,1024]{1,0:T(8,128)(2,1)} %get-tuple-element.8) | data formatting | bytes 1048576
  92.7 1.6 %copy.18 = bf16[256,256]{1,0:T(8,128)(2,1)} copy(bf16[256,256]{1,0:T(8,128)(2,1)} %get-tuple-element.9) | data formatting | bytes 262144
  94.2 1.6 %copy.19 = bf16[256,256]{1,0:T(8,128)(2,1)} copy(bf16[256,256]{1,0:T(8,128)(2,1)} %get-tuple-element.10) | data formatting | bytes 262144
  95.8 1.9 %copy.20 = f32[512,256]{1,0:T(8,128)} copy(f32[512,256]{1,0:T(8,128)} %get-tuple-element.11) | data formatting | bytes 1048576

commit v4 on v3

--- a/solution.py
+++ b/solution.py
@@ -378,6 +378,11 @@
                 down_copy(ob, part).wait_send()
 
 
+def write_kernel(*refs):
+    for src, dst in zip(refs[:4], refs[4:]):
+        dst[...] = src[...]
+
+
 def on_device(n, tp_count, hidden, key_weight, queries, values, map_out, log_sums, out_grad, mixing, out_gain):
     rows = queries.shape[0]
     heads = mixing.shape[0]
@@ -386,7 +391,7 @@
     outer = n // 2
     vm = pl.BlockSpec(memory_space=VMEM)
     hops = pltpu.SemaphoreType.DMA((outer, 2))
-    return pl.pallas_call(
+    results = pl.pallas_call(
         functools.partial(attend_kernel, n, tp_count, heads, groups),
         out_shape=(
             jax.ShapeDtypeStruct(queries.shape, jnp.bfloat16),
@@ -417,6 +422,13 @@
         ),
         cost_estimate=pl.CostEstimate(flops=5 * 10**9, bytes_accessed=10**7, transcendentals=0),
     )(hidden, key_weight, values, queries, map_out, out_grad, log_sums, out_gain.reshape(1, V_DIM), mixing)
+    return pl.pallas_call(
+        write_kernel,
+        out_shape=tuple(jax.ShapeDtypeStruct(r.shape, r.dtype) for r in results),
+        in_specs=[vm] * 4,
+        out_specs=(vm,) * 4,
+        cost_estimate=pl.CostEstimate(flops=10**6, bytes_accessed=4 * 10**6, transcendentals=0),
+    )(*results)
 
 
 def solution(mesh):

time: 97.9 us -> 93.3 us (0.953)
  local copies, waits for them, and re-layouts: 6.87 us -> 0 us
  Pallas kernels: 90.2 us -> 92.5 us
    unnamed x4 -> x0, local copies, waits for them, and re-layouts: 6.87 us -> none
    pallas_call x0 -> x1, Pallas kernels: none -> 2.38 us  [on_device(): pl.pallas_call(write_kernel, out_shape=tuple((jax.ShapeDtypeStruct(r.shap...]
where the time goes in v4:
time: 93.3 us; the launch traced here: 93.2 us
  Pallas kernels  92.5 us (99%)
    pallas_call x1, Pallas kernels, on_device(): pl.pallas_call(functools.partial(attend_kernel, n, tp_count, heads, group...  90.2 us
    pallas_call x1, Pallas kernels, on_device(): pl.pallas_call(write_kernel, out_shape=tuple((jax.ShapeDtypeStruct(r.shap...  2.38 us

profile of v4, /device:TPU:29, one launch (start us, length us, event | category | flops | bytes accessed | tf_op | source)
XLA Modules:
  0.0 93.2 jit_solution(8621474142234497390)
XLA Ops:
  0.6 90.2 %shard_map.120 = (bf16[256,1024]{1,0:T(8,128)(2,1)}, bf16[256,256]{1,0:T(8,128)(2,1)}, bf16[256,256]{1,0:T(8,128)(2,1)}, f32[512,256]{1,0:T(8,128)}) custom-call(bf16[256,4096]{1,0:T(8,128)(2,1)} %hidden_ref.1, bf16[4096,256]{1,0:T(8,128)(2,1)} %weight_ref.1, bf16[256,256]{1,0:T(8,128)(2,1)} %values_ref.1, bf16[256,1024]{1,0:T(8,128)(2,1)} %q_ref.1, ...), custom_call_target="tpu_custom_call" | custom-call | flops 5000000000 | bytes 10000000 | tf_op jit(solution)/shard_map/pallas_call | solution.py:394
  90.8 2.4 %shard_map.121 = (bf16[256,1024]{1,0:T(8,128)(2,1)}, bf16[256,256]{1,0:T(8,128)(2,1)}, bf16[256,256]{1,0:T(8,128)(2,1)}, f32[512,256]{1,0:T(8,128)}) custom-call(bf16[256,1024]{1,0:T(8,128)(2,1)} %get-tuple-element.8.refs_0_, bf16[256,256]{1,0:T(8,128)(2,1)} %get-tuple-element.9.refs_1_, bf16[256,256]{1,0:T(8,128)(2,1)} %get-tuple-element.10.refs_2_, ...), custom_call_target="tpu_custom_call" | custom-call | flops 1000000 | bytes 4000000 | tf_op jit(solution)/shard_map/pallas_call | solution.py:425

commit v5 on v4

--- a/solution.py
+++ b/solution.py
@@ -98,8 +98,8 @@
     n, tp_count, heads, groups,
     hidden_ref, weight_ref, values_ref, q_ref, mo_ref, og_ref, log_ref, gain_ref, mix_ref,
     gq_out, gk_out, gv_out, gw_out,
-    d_ref, term_ref, gq_ref, kv_ref, acc_ref, side_out, side_in, down_out, up_in, hid_ref, gk_ref,
-    kv_recv, kv_up_sem, kv_side_sem, side_send, side_recv, down_send, up_recv,
+    d_ref, term_ref, gq_ref, kv_ref, acc_ref, side_out, side_in, down_out, up_in, up_side, hid_ref, gk_ref,
+    kv_recv, kv_up_sem, kv_side_sem, side_send, side_recv, down_send, up_recv, cross_send, cross_recv,
     hid_send, hid_pass, hid_recv, gk_recv, gk_up_sem, gk_down_sem, gk_side_sem,
 ):
     me = lax.axis_index("sp")
@@ -112,7 +112,7 @@
         return pltpu.make_async_remote_copy(
             src_ref=kv_ref.at[b, part] if src is None else src,
             dst_ref=kv_ref.at[b, part],
-            send_sem=sems.at[b // 2, part],
+            send_sem=sems.at[b, part],
             recv_sem=kv_recv.at[b, part],
             device_id={"sp": target},
         )
@@ -132,6 +132,15 @@
             dst_ref=up_in.at[ob, part],
             send_sem=down_send.at[ob, part],
             recv_sem=up_recv.at[ob, part],
+            device_id={"sp": down},
+        )
+
+    def cross_copy(ob):
+        return pltpu.make_async_remote_copy(
+            src_ref=side_out.at[ob, 1],
+            dst_ref=up_side.at[ob],
+            send_sem=cross_send.at[ob],
+            recv_sem=cross_recv.at[ob],
             device_id={"sp": down},
         )
 
@@ -219,7 +228,7 @@
         def _():
             kv_copy(me, part, kv_up_sem, up, src).start()
 
-        @pl.when(y == 0)
+        @pl.when((y == 0) | (has_up & (part == 1)))
         def _():
             kv_copy(me, part, kv_side_sem, side, src).start()
 
@@ -267,18 +276,25 @@
                 def _():
                     kv_copy(b, part, kv_up_sem, up).start()
 
-                kv_copy(b, part, kv_side_sem, side).start()
+                if part == 0:
+                    kv_copy(b, part, kv_side_sem, side).start()
             store(acc_ref, o - t, grads(b, False))
 
-        @pl.when((t > 0) & (t <= o + 1) & ((t > 1) | (y == 1)))
+        @pl.when((t > 0) & (t <= o + 1) & ((t > 1) | (y == 1) | has_up))
         def _():
             ob = o - t + 1
             b = 2 * ob + 1 - y
-            for part in (1, 0):
-                kv_copy(b, part, kv_side_sem, side).wait_recv()
-            store(side_out, ob, grads(b, False))
-            for part in range(2):
-                side_copy(ob, part).start()
+            kv_copy(b, 1, kv_side_sem, side).wait_recv()
+
+            @pl.when(has_up)
+            def _():
+                kv_copy(b, 1, kv_up_sem, up).start()
+
+            @pl.when((t > 1) | (y == 1))
+            def _():
+                kv_copy(b, 0, kv_side_sem, side).wait_recv()
+                store(side_out, ob, grads(b, False))
+                side_copy(ob, 0).start()
 
         @pl.when((t == o + 1) & has_up)
         def _():
@@ -292,7 +308,29 @@
         def _():
             ob = o - t + lag
             for part in range(2):
-                @pl.when((ob < o) | (y == 0))
+                if part == 1:
+                    @pl.when(has_up)
+                    def _():
+                        cross_copy(ob).wait_recv()
+
+                        @pl.when((ob < o) | (y == 1))
+                        def _():
+                            total = side_out[ob, 1].astype(jnp.float32) + up_side[ob].astype(jnp.float32)
+                            side_out[ob, 1] = total.astype(jnp.bfloat16)
+
+                        @pl.when((ob == o) & (y == 0))
+                        def _():
+                            side_out[ob, 1] = up_side[ob]
+
+                    @pl.when(ob < o)
+                    def _():
+                        cross_copy(ob).start()
+
+                    @pl.when((ob == o) & ((y == 1) | has_up))
+                    def _():
+                        side_copy(ob, 1).start()
+
+                @pl.when(((ob < o) | (y == 0)) if part == 0 else ((ob == o) & ((y == 0) | has_up)))
                 def _():
                     side_copy(ob, part).wait_recv()
                     acc_ref[ob, part] += side_in[ob, part].astype(jnp.float32)
@@ -360,22 +398,33 @@
 
     @pl.loop(0, o + 1)
     def _(ob):
-        for part in range(2):
-            @pl.when(has_up)
-            def _():
+        @pl.when(has_up)
+        def _():
+            for part in range(2):
                 kv_copy(2 * ob + y, part, kv_up_sem, up).wait_send()
-
-            @pl.when((ob < o) | (y == 0))
-            def _():
-                kv_copy(2 * ob + y, part, kv_side_sem, side).wait_send()
-
-            @pl.when((ob < o) | (y == 1))
-            def _():
-                side_copy(ob, part).wait_send()
-
-            @pl.when(ob < o)
-            def _():
+            kv_copy(2 * ob + 1 - y, 1, kv_up_sem, up).wait_send()
+
+        @pl.when((ob < o) | (y == 0))
+        def _():
+            kv_copy(2 * ob + y, 0, kv_side_sem, side).wait_send()
+
+        @pl.when((ob < o) | (y == 1))
+        def _():
+            side_copy(ob, 0).wait_send()
+
+        @pl.when(ob < o)
+        def _():
+            for part in range(2):
                 down_copy(ob, part).wait_send()
+            cross_copy(ob).wait_send()
+
+    @pl.when((y == 0) | has_up)
+    def _():
+        kv_copy(me, 1, kv_side_sem, side).wait_send()
+
+    @pl.when((y == 1) | has_up)
+    def _():
+        side_copy(o, 1).wait_send()
 
 
 def write_kernel(*refs):
@@ -410,11 +459,13 @@
         ]
         + [VMEM((outer, 2, rows, width), jnp.bfloat16)] * 4
         + [
+            VMEM((outer, rows, width), jnp.bfloat16),
             VMEM((tp_count, n, rows // tp_count, hidden.shape[1] // n), jnp.bfloat16),
             VMEM((n, rows, width), jnp.bfloat16),
         ]
-        + [pltpu.SemaphoreType.DMA((n, 2))]
-        + [hops] * 6
+        + [pltpu.SemaphoreType.DMA((n, 2))] * 3
+        + [hops] * 4
+        + [pltpu.SemaphoreType.DMA((outer,))] * 2
         + [pltpu.SemaphoreType.DMA]
         + [pltpu.SemaphoreType.DMA((size,)) for size in (tp_count, tp_count, n, outer, outer, outer)],
         compiler_params=pltpu.CompilerParams(

time: 93.3 us -> 94.4 us (1.012)
  the two profiles are of different devices: /device:TPU:29 before, /device:TPU:0 now
where the time goes in v5:
time: 94.4 us; the launch traced here: 94.3 us
  Pallas kernels  93.6 us (99%)
    pallas_call x1, Pallas kernels, on_device(): pl.pallas_call(functools.partial(attend_kernel, n, tp_count, heads, group...  91.2 us
    pallas_call x1, Pallas kernels, on_device(): pl.pallas_call(write_kernel, out_shape=tuple((jax.ShapeDtypeStruct(r.shap...  2.38 us

profile of v5, /device:TPU:0, one launch (start us, length us, event | category | flops | bytes accessed | tf_op | source)
XLA Modules:
  0.0 94.3 jit_solution(13449257070725678169)
XLA Ops:
  0.6 91.2 %shard_map.120 = (bf16[256,1024]{1,0:T(8,128)(2,1)}, bf16[256,256]{1,0:T(8,128)(2,1)}, bf16[256,256]{1,0:T(8,128)(2,1)}, f32[512,256]{1,0:T(8,128)}) custom-call(bf16[256,4096]{1,0:T(8,128)(2,1)} %hidden_ref.1, bf16[4096,256]{1,0:T(8,128)(2,1)} %weight_ref.1, bf16[256,256]{1,0:T(8,128)(2,1)} %values_ref.1, bf16[256,1024]{1,0:T(8,128)(2,1)} %q_ref.1, ...), custom_call_target="tpu_custom_call" | custom-call | flops 5000000000 | bytes 10000000 | tf_op jit(solution)/shard_map/pallas_call | solution.py:443
  91.9 2.4 %shard_map.121 = (bf16[256,1024]{1,0:T(8,128)(2,1)}, bf16[256,256]{1,0:T(8,128)(2,1)}, bf16[256,256]{1,0:T(8,128)(2,1)}, f32[512,256]{1,0:T(8,128)}) custom-call(bf16[256,1024]{1,0:T(8,128)(2,1)} %get-tuple-element.8.refs_0_, bf16[256,256]{1,0:T(8,128)(2,1)} %get-tuple-element.9.refs_1_, bf16[256,256]{1,0:T(8,128)(2,1)} %get-tuple-element.10.refs_2_, ...), custom_call_target="tpu_custom_call" | custom-call | flops 1000000 | bytes 4000000 | tf_op jit(solution)/shard_map/pallas_call | solution.py:476
